TPU v7x, 512 devices: a whole 4x4x16 slice. The times are simulated.
512 devices in a mesh: ep: 32 (over z, core), tp: 16 (over y, x).
Axes of the slice: x: 4, y: 4, z: 16, core: 2. Of those that a mesh axis runs over, the one named last changes fastest.
Arguments:
- mix_in: bfloat16 [4096, 2048], P('ep'), may hold values from -6 to 6
- mix_gain: float32 [2048], replicated, may hold values from 0.1 to 1.9
- lam_re: float32 [128, 64], P('tp'), may hold values from -0.34 to -1e-05
- lam_im: float32 [128, 64], P('tp'), may hold values from 0.2 to 4
- log_dt: float32 [128], P('tp'), may hold values from -2.31 to 0
- b_re: float32 [128, 64, 16], P('tp'), may hold values from -0.0625 to 0.0625
- b_im: float32 [128, 64, 16], P('tp'), may hold values from -0.0625 to 0.0625
- c_re: float32 [128, 16, 64], P('tp'), may hold values from -0.5 to 0.5
- c_im: float32 [128, 16, 64], P('tp'), may hold values from -0.5 to 0.5
- d_skip: float32 [2048], P('tp'), may hold values from -2 to 2
- log_retain: float32 [4096, 128], P('ep', 'tp'), may hold values from -2.2 to 0
- w_lin: bfloat16 [2048, 2048], P(None, 'tp'), may hold values from -0.125 to 0.125
- w_glu: bfloat16 [2048, 2048], P(None, 'tp'), may hold values from -0.125 to 0.125
- moe_in: bfloat16 [4096, 2048], P('ep'), may hold values from -6 to 6
- moe_gain: float32 [2048], replicated, may hold values from 0.1 to 1.9
- routes: int32 [4096, 2], P('ep'), may hold values from 0 to 31, all different within a row; in each aligned block of 128 rows (0 to 127, 128 to 255, ...) at most 12 rows name the same one
- route_weight: float32 [4096, 2], P('ep'), may hold values from 0.1 to 1
- w_gate: bfloat16 [32, 2048, 4096], P('ep', None, 'tp'), may hold values from -0.125 to 0.125
- w_up: bfloat16 [32, 2048, 4096], P('ep', None, 'tp'), may hold values from -0.125 to 0.125
- w_down: bfloat16 [32, 4096, 2048], P('ep', 'tp'), may hold values from -0.09375 to 0.09375
Outputs:
- mix_out: bfloat16 [4096, 2048], P('ep', 'tp')
- moe_out: bfloat16 [4096, 2048], P('ep', 'tp')
Inputs may be any that keep to these rules, and one draw needn't show every extreme that they name: `routes`: each row names 2 different experts. In each aligned block of 128 rows (the rows of one index of ep) no expert is named by more than 12 rows, and in some block an expert is named by exactly 12 rows.
All inputs are finite; a program needn't handle non-finite values.
Results may differ from a plain program's by a relative error of at most 0.015.
Values may be sent and summed in bfloat16 or wider, within the bound.
A program may use at most 128 MiB of HBM per device.

v0:
```python
import jax
import jax.numpy as jnp
from jax import lax
from jax.sharding import Mesh
from jax.sharding import PartitionSpec as P

EP = ("ep_0", "ep_1")


EPS = 1e-06
HIGHEST = lax.Precision.HIGHEST


def filled_with(array, identity):
    return jax.tree.map(
        lambda part, zero: jnp.zeros_like(part) + jnp.asarray(zero, part.dtype), array, identity
    )


def all_in_one(array, axis):
    leaves = jax.tree.leaves(array)
    order = sorted(range(len(leaves)), key=lambda k: -leaves[k].size)
    width = (1, *leaves[order[0]].shape)[-1]
    lines = [
        jnp.pad(leaves[k].reshape(-1), (0, -leaves[k].size % width)).reshape(-1, width)
        for k in order
    ]
    both, at, found = (lax.all_gather(jnp.concatenate(lines), axis), 0, {})
    for k, line in zip(order, lines):
        slab = both[:, at : at + len(line)].reshape(len(both), -1)
        found[k] = slab[:, : leaves[k].size].reshape(-1, *leaves[k].shape)
        at += len(line)
    numbers = iter(range(len(leaves)))
    return jax.tree.map(lambda _: found[next(numbers)], array)


def entering(array, axes, combine, identity):
    before = start = filled_with(array, identity)
    subtotal = array
    for axis in reversed(axes):
        length, here = (lax.axis_size(axis), lax.axis_index(axis))
        pieces = all_in_one(subtotal, axis)
        inside, subtotal = (start, start)
        for k in range(length):
            passed = k < here
            subtotal = combine(subtotal, jax.tree.map(lambda part: part[k], pieces))
            inside = jax.tree.map(lambda new, old: jnp.where(passed, new, old), subtotal, inside)
        before = combine(inside, before)
    return before


def laid_out(pieces, dim):
    lengths = list(pieces.shape[1:])
    lengths[dim] *= pieces.shape[0]
    return jnp.moveaxis(pieces, 0, dim).reshape(lengths)


def from_everyone(array, axis):
    copies = jnp.broadcast_to(array, (lax.axis_size(axis), *array.shape))
    return lax.all_to_all(copies, axis, split_axis=0, concat_axis=0, tiled=True)


def gather_directly(array, axis, dim):
    return laid_out(from_everyone(array, axis), dim)


def in_blocks(array, dim, length):
    before, after = (array.shape[:dim], array.shape[dim + 1 :])
    return jnp.moveaxis(array.reshape(*before, length, -1, *after), dim, 0)


def sent_and_summed(array, axis, dim):
    pieces = in_blocks(array, dim, lax.axis_size(axis))
    arrived = lax.all_to_all(pieces, axis, split_axis=0, concat_axis=0, tiled=True)
    return arrived.astype(jnp.float32).sum(axis=0)


def root_mean_normed(values, gain):
    broadened_rows = values.astype(jnp.float32)
    inverse = lax.rsqrt(jnp.mean(broadened_rows * broadened_rows, axis=-1, keepdims=True) + EPS)
    return (broadened_rows * inverse * gain).astype(jnp.bfloat16)


def compose(earlier, later):
    early_re, early_im, shift_re, shift_im = earlier
    late_re, late_im, offset_re, offset_im = later
    return (
        late_re * early_re - late_im * early_im,
        late_re * early_im + late_im * early_re,
        late_re * shift_re - late_im * shift_im + offset_re,
        late_re * shift_im + late_im * shift_re + offset_im,
    )


def discretize(lam_re, lam_im, log_dt, b_re, b_im):
    time_step = jnp.exp(log_dt)[:, None]
    log_mag = lam_re * time_step
    angle = lam_im * time_step
    half_sine = jnp.sin(0.5 * angle)
    minus_re = jnp.expm1(log_mag) * jnp.cos(angle) - 2.0 * half_sine * half_sine
    minus_im = jnp.exp(log_mag) * jnp.sin(angle)
    denom = lam_re * lam_re + lam_im * lam_im
    coef_re = (minus_re * lam_re + minus_im * lam_im) / denom
    coef_im = (minus_im * lam_re - minus_re * lam_im) / denom
    drive_re = coef_re[..., None] * b_re - coef_im[..., None] * b_im
    drive_im = coef_re[..., None] * b_im + coef_im[..., None] * b_re
    return (log_mag, angle, drive_re, drive_im)


def block_scan(inputs, retain, log_mag, angle, drive_re, drive_im):
    length = inputs.shape[0]
    groups, states, channels = drive_re.shape
    broadened_rows = inputs.astype(jnp.float32).reshape(length, groups, channels)
    push_re = jnp.einsum("tgn,gpn->gtp", broadened_rows, drive_re, precision=HIGHEST)
    push_im = jnp.einsum("tgn,gpn->gtp", broadened_rows, drive_im, precision=HIGHEST)
    steps = jnp.arange(length, dtype=jnp.float32)
    causal = steps[:, None] >= steps[None, :]
    summed = jnp.dot(causal.astype(jnp.float32), retain, precision=HIGHEST)
    rows = summed.T
    gaps = jnp.minimum(rows[:, :, None] - rows[:, None, :], 0.0)
    kept = jnp.where(causal[None], jnp.exp(gaps), 0.0)
    centred = (steps - length // 2)[None, :, None]
    growth = log_mag[:, None, :] * centred
    turn = angle[:, None, :] * centred
    cosine = jnp.cos(turn)
    sine = jnp.sin(turn)
    up_re = jnp.exp(growth) * cosine
    up_im = jnp.exp(growth) * sine
    down_re = jnp.exp(-growth) * cosine
    down_im = -jnp.exp(-growth) * sine
    seed_re = push_re * down_re - push_im * down_im
    seed_im = push_re * down_im + push_im * down_re
    seeds = jnp.concatenate([seed_re, seed_im], axis=2)
    held = jnp.einsum("gts,gsp->gtp", kept, seeds, precision=HIGHEST)
    fade = jnp.exp(rows)[:, :, None]
    return (held[..., :states], held[..., states:], up_re, up_im, fade)


def power_of(log_mag, angle, exponent):
    magnitude = jnp.exp(log_mag * exponent)
    return (magnitude * jnp.cos(angle * exponent), magnitude * jnp.sin(angle * exponent))


def read_out(state_re, state_im, inputs, c_re, c_im, d_skip):
    length = inputs.shape[0]
    groups, channels, states = c_re.shape
    states_both = jnp.concatenate([state_re, state_im], axis=2)
    c_both = jnp.concatenate([c_re, -c_im], axis=2)
    mixed = jnp.einsum("gtp,gnp->tgn", states_both, c_both, precision=HIGHEST)
    skipped = mixed.reshape(length, groups * channels) + d_skip * inputs.astype(jnp.float32)
    return jax.nn.gelu(skipped).astype(jnp.bfloat16)


def local(
    mix_in,
    mix_gain,
    lam_re,
    lam_im,
    log_dt,
    b_re,
    b_im,
    c_re,
    c_im,
    d_skip,
    log_retain,
    w_lin,
    w_glu,
    moe_in,
    moe_gain,
    routes,
    route_weight,
    w_gate,
    w_up,
    w_down,
):
    normed = root_mean_normed(mix_in, mix_gain)
    channels_here = d_skip.shape[0]
    own_inputs = lax.dynamic_slice_in_dim(
        normed, lax.axis_index("tp") * channels_here, channels_here, 1
    )
    log_mag, angle, drive_re, drive_im = discretize(lam_re, lam_im, log_dt, b_re, b_im)
    held_re, held_im, up_re, up_im, fade = block_scan(
        own_inputs, log_retain, log_mag, angle, drive_re, drive_im
    )
    length = own_inputs.shape[0]
    end_re = (up_re * held_re - up_im * held_im)[:, -1]
    end_im = (up_re * held_im + up_im * held_re)[:, -1]
    whole_re, whole_im = power_of(log_mag, angle, float(length))
    pref_re = fade[:, -1] * whole_re
    pref_im = fade[:, -1] * whole_im
    flat = [part.reshape(-1) for part in (pref_re, pref_im, end_re, end_im)]
    unity = jnp.ones_like(flat[0])
    nought = jnp.zeros_like(flat[0])
    incoming = entering(tuple(flat), EP, compose, (unity, nought, nought, nought))
    carry_re = incoming[2].reshape(pref_re.shape)
    carry_im = incoming[3].reshape(pref_re.shape)
    lead_re, lead_im = power_of(log_mag, angle, float(length // 2 + 1))
    first_re = lead_re * carry_re - lead_im * carry_im
    first_im = lead_re * carry_im + lead_im * carry_re
    held_re = held_re + fade * first_re[:, None, :]
    held_im = held_im + fade * first_im[:, None, :]
    total_re = up_re * held_re - up_im * held_im
    total_im = up_re * held_im + up_im * held_re
    activated = read_out(total_re, total_im, own_inputs, c_re, c_im, d_skip)
    piece = gather_directly(activated, "tp", 1)
    mix_lin = jnp.dot(piece, w_lin, preferred_element_type=jnp.float32)
    mix_glu = jnp.dot(piece, w_glu, preferred_element_type=jnp.float32)
    mix_out = (mix_lin * jax.nn.sigmoid(mix_glu)).astype(jnp.bfloat16)
    normed_b = root_mean_normed(moe_in, moe_gain)
    experts = lax.axis_size(EP)
    tokens_here, choices_each = routes.shape
    capacity = 3 * choices_each * tokens_here // (2 * experts)
    flat_routes = routes.reshape(-1)
    onehot = (flat_routes[:, None] == jnp.arange(experts, dtype=jnp.int32)[None, :]).astype(
        jnp.int32
    )
    earlier_count = jnp.cumsum(onehot, axis=0) - onehot
    slot_index = jnp.sum(earlier_count * onehot, axis=1)
    target = flat_routes * capacity + slot_index
    places = jnp.arange(experts * capacity, dtype=jnp.int32)
    picked = jnp.any(
        places[:, None, None] == target.reshape(tokens_here, choices_each)[None], axis=2
    )
    picked = picked.astype(jnp.bfloat16)
    outgoing = jnp.dot(picked, normed_b, preferred_element_type=jnp.float32).astype(jnp.bfloat16)
    outgoing = outgoing.reshape(experts, capacity, normed_b.shape[1])
    gate_local = w_gate[0]
    up_local = w_up[0]
    down_local = w_down[0]
    received = lax.all_to_all(outgoing, EP, split_axis=0, concat_axis=0, tiled=True)
    senders, slots_here, features_here = received.shape
    token_rows = received.reshape(senders * slots_here, features_here)
    gate_pre = jnp.dot(token_rows, gate_local, preferred_element_type=jnp.float32)
    up_pre = jnp.dot(token_rows, up_local, preferred_element_type=jnp.float32)
    hidden = (jax.nn.silu(gate_pre) * up_pre).astype(jnp.bfloat16)
    partial_out = jnp.dot(hidden, down_local, preferred_element_type=jnp.float32).astype(
        jnp.bfloat16
    )
    partial_out = lax.optimization_barrier(partial_out)
    summed = sent_and_summed(partial_out.astype(jnp.float32).astype(jnp.bfloat16), "tp", 1)
    final_result = summed.astype(jnp.bfloat16).reshape(senders, slots_here, summed.shape[1])
    returned = lax.all_to_all(final_result, EP, split_axis=0, concat_axis=0, tiled=True)
    flat_returned = returned.reshape(experts * capacity, returned.shape[2])
    gathered = (
        flat_returned[target]
        .astype(jnp.float32)
        .reshape(tokens_here, choices_each, returned.shape[2])
    )
    moe_out = jnp.sum(gathered * route_weight[:, :, None], axis=1).astype(jnp.bfloat16)
    return (mix_out, moe_out)


def solution(mesh):
    torus = Mesh(mesh.devices.reshape(16, 2, mesh.shape["tp"]), ("ep_0", "ep_1", "tp"))
    placed = (
        P(EP, None),
        P(),
        P("tp", None),
        P("tp", None),
        P("tp"),
        P("tp", None, None),
        P("tp", None, None),
        P("tp", None, None),
        P("tp", None, None),
        P("tp"),
        P(EP, "tp"),
        P(None, "tp"),
        P(None, "tp"),
        P(EP, None),
        P(),
        P(EP, None),
        P(EP, None),
        P(EP, None, "tp"),
        P(EP, None, "tp"),
        P(EP, "tp", None),
    )
    return jax.shard_map(
        local, mesh=torus, in_specs=placed, out_specs=(P(EP, "tp"), P(EP, "tp")), check_vma=False
    )
```

profile of v0, /device:TPU:1, one launch (start us, length us, event | category | flops | bytes accessed | tf_op | source)
XLA Modules:
  0.0 247.5 jit_solution(3403448465952163818)
XLA Ops:
  0.7 0.9 copy.50
  3.7 1.2 fusion.6
  4.9 1.3 convolution_convert_fusion.1
  6.3 1.5 reshape.691
  7.8 16.7 %all-to-all-start.1 = ((bf16[32,12,2048]{2,1,0:T(8,128)(2,1)}), bf16[32,12,2048]{2,1,0:T(8,128)(2,1)S(1)}, u32[]{:S(2)}, u32[]{:S(2)}) async-start(bf16[32,12,2048]{2,1,0:T(8,128)(2,1)} %reshape.691), calls=%async_computation.1 | async-start | bytes 4194304 | tf_op jit(solution)/shard_map/all_to_all | solution.py:230
  24.6 2.2 convert_element_type.54
  26.8 0.8 dynamic-slice
  27.6 1.2 multiply_reduce_fusion
  29.3 0.9 fusion.62
  31.4 1.4 fusion.43
  32.8 1.3 fusion.15
  34.2 0.8 copy-done.2
  35.9 1.8 all-gather.2
  37.8 97.6 %all-gather.3 = f32[16,4,512]{2,1,0:T(4,128)S(1)} all-gather(f32[1,4,512]{2,1,0:T(4,128)S(1)} %maximum_bitcast_fusion.1), channel_id=3, replica_groups=mesh['ep_0'=16,'ep_1'=2,'tp'=16] {'ep_0'}, dimensions={0}, use_global_device_ids=true | all-gather | bytes 139264 | tf_op jit(solution)/shard_map/all_gather | solution.py:28
  137.0 0.7 squeeze.300
  137.7 0.7 reshape.753
  139.1 0.7 squeeze.251
  140.4 0.7 squeeze.269
  141.7 0.7 squeeze.271
  143.1 0.7 squeeze.273
  143.7 0.7 squeeze.274
  145.0 0.7 squeeze.293
  146.4 0.7 squeeze.295
  147.0 0.7 squeeze.296
  148.4 0.7 squeeze.298
  149.0 1.3 reshape.692
  150.4 2.4 fusion.12
  152.8 4.2 %convolution_convert_fusion = bf16[384,2048]{1,0:T(8,128)(2,1)} fusion(bf16[384,2048]{1,0:T(8,128)(2,1)S(1)} %copy-done.4, bf16[1,256,2048]{2,1,0:T(8,128)(2,1)S(1)} %copy-done, bf16[1,2048,256]{2,1,0:T(8,128)(2,1)} %param.38, f32[384,256]{1,0:T(8,128)S(1)} %fusion.12), kind=kOutput, calls=%fused_computation.1 | convolution fusion | flops 806682624 | bytes 5636096 | tf_op jit(solution)/shard_map/dot_general | solution.py:236
  157.0 3.0 %bitcast_bitcast_fusion = bf16[16,384,128]{2,1,0:T(8,128)(2,1)} fusion(bf16[384,2048]{1,0:T(8,128)(2,1)} %convolution_convert_fusion), kind=kLoop, calls=%fused_computation.3 | loop fusion | bytes 3145728 | tf_op jit(solution)/shard_map/transpose | solution.py:69
  159.9 6.9 %all-to-all-start.2 = ((bf16[16,384,128]{2,1,0:T(8,128)(2,1)}), bf16[16,384,128]{2,1,0:T(8,128)(2,1)S(1)}, u32[]{:S(2)}, u32[]{:S(2)}) async-start(bf16[16,384,128]{2,1,0:T(8,128)(2,1)} %bitcast_bitcast_fusion), calls=%async_computation.2 | async-start | bytes 3145728 | tf_op jit(solution)/shard_map/all_to_all | solution.py:74
  166.8 0.7 slice_reduce_fusion.3
  167.6 0.8 squeeze.275
  168.3 0.8 squeeze.276
  169.1 0.7 squeeze.277
  169.8 0.7 squeeze.278
  170.5 0.7 squeeze.279
  171.3 0.8 squeeze.280
  172.0 0.7 squeeze.281
  172.8 0.7 squeeze.282
  173.5 1.3 squeeze.283
  174.8 1.3 squeeze.284
  176.2 1.3 squeeze.285
  177.5 1.3 squeeze.286
  178.8 1.3 squeeze.287
  180.2 1.3 squeeze.288
  181.5 1.3 squeeze.289
  182.9 1.3 squeeze.290
  184.2 1.3 squeeze.291
  185.5 1.3 squeeze.299
  186.9 1.3 reshape.758
  188.9 1.1 multiply_subtract_fusion.1
  190.0 0.7 multiply_add_fusion.3
  190.7 1.9 multiply_subtract_fusion
  193.4 1.0 fusion.60
  194.5 0.9 broadcast_in_dim.28
  195.4 6.7 %all-to-all-start = ((bf16[16,128,128]{1,2,0:T(8,128)(2,1)}), bf16[16,128,128]{1,2,0:T(8,128)(2,1)S(1)}, u32[]{:S(2)}, u32[]{:S(2)}) async-start(bf16[16,128,128]{1,2,0:T(8,128)(2,1)} %broadcast_in_dim.28), calls=%async_computation | async-start | bytes 1048576 | tf_op jit(solution)/shard_map/all_to_all | solution.py:60
  202.6 0.7 reshape.694
  203.3 7.8 %all-to-all-done = bf16[16,128,128]{1,2,0:T(8,128)(2,1)S(1)} async-done(((bf16[16,128,128]{1,2,0:T(8,128)(2,1)}), bf16[16,128,128]{1,2,0:T(8,128)(2,1)S(1)}, u32[]{:S(2)}, u32[]{:S(2)}) %all-to-all-start) | async-done | bytes 524320 | tf_op jit(solution)/shard_map/all_to_all | solution.py:60
  211.1 18.8 %all-to-all-start.3 = ((bf16[32,12,128]{2,1,0:T(8,128)(2,1)}), bf16[32,12,128]{2,1,0:T(8,128)(2,1)S(1)}, u32[]{:S(2)}, u32[]{:S(2)}) async-start(bf16[32,12,128]{2,1,0:T(8,128)(2,1)} %reshape.694), calls=%async_computation.3 | async-start | bytes 262144 | tf_op jit(solution)/shard_map/all_to_all | solution.py:242
  229.9 1.4 fusion.97
  231.3 1.0 fusion.5
  232.2 13.5 %all-to-all-done.3 = bf16[32,12,128]{2,1,0:T(8,128)(2,1)S(1)} async-done(((bf16[32,12,128]{2,1,0:T(8,128)(2,1)}), bf16[32,12,128]{2,1,0:T(8,128)(2,1)S(1)}, u32[]{:S(2)}, u32[]{:S(2)}) %all-to-all-start.3) | async-done | bytes 98336 | tf_op jit(solution)/shard_map/all_to_all | solution.py:242
  245.7 0.9 gather_fusion
  246.6 0.9 fusion.52
  (119 shorter events, 13.0 us)
Async XLA Ops:
  0.6 152.1 %copy-start = (bf16[1,256,2048]{2,1,0:T(8,128)(2,1)S(1)}, bf16[1,256,2048]{2,1,0:T(8,128)(2,1)}, u32[]{:S(2)}) copy-start(bf16[1,256,2048]{2,1,0:T(8,128)(2,1)} %param.39) | copy-start | bytes 3145732
  0.6 4.3 %copy-start.1 = (bf16[128,2048]{1,0:T(8,128)(2,1)S(1)}, bf16[128,2048]{1,0:T(8,128)(2,1)}, u32[]{:S(2)}) copy-start(bf16[128,2048]{1,0:T(8,128)(2,1)} %param.33) | copy-start | bytes 1572868
  2.8 0.6 copy-start.12
  7.8 141.2 %all-to-all-start.1 = ((bf16[32,12,2048]{2,1,0:T(8,128)(2,1)}), bf16[32,12,2048]{2,1,0:T(8,128)(2,1)S(1)}, u32[]{:S(2)}, u32[]{:S(2)}) async-start(bf16[32,12,2048]{2,1,0:T(8,128)(2,1)} %reshape.691), calls=%async_computation.1 | async-start | bytes 4194304 | tf_op jit(solution)/shard_map/all_to_all | solution.py:230
  24.6 5.8 %copy-start.20 = (f32[8]{0:T(128)S(1)}, f32[8]{0:T(128)}, u32[]{:S(2)}) copy-start(f32[8]{0:T(128)} %param.24) | copy-start | bytes 100
  24.6 5.8 %copy-start.19 = (f32[128,8]{0,1:T(8,128)S(1)}, f32[128,8]{0,1:T(8,128)}, u32[]{:S(2)}) copy-start(f32[128,8]{0,1:T(8,128)} %param.30) | copy-start | bytes 12292
  24.6 6.3 %copy-start.10 = (f32[8,64]{1,0:T(8,128)S(1)}, f32[8,64]{1,0:T(8,128)}, u32[]{:S(2)}) copy-start(f32[8,64]{1,0:T(8,128)} %param.22) | copy-start | bytes 6148
  24.6 6.3 %copy-start.11 = (f32[8,64]{1,0:T(8,128)S(1)}, f32[8,64]{1,0:T(8,128)}, u32[]{:S(2)}) copy-start(f32[8,64]{1,0:T(8,128)} %param.23) | copy-start | bytes 6148
  24.6 6.4 %copy-start.6 = (f32[8,64,16]{1,2,0:T(8,128)S(1)}, f32[8,64,16]{1,2,0:T(8,128)}, u32[]{:S(2)}) copy-start(f32[8,64,16]{1,2,0:T(8,128)} %param.25) | copy-start | bytes 98308
  24.6 6.4 %copy-start.7 = (f32[8,64,16]{1,2,0:T(8,128)S(1)}, f32[8,64,16]{1,2,0:T(8,128)}, u32[]{:S(2)}) copy-start(f32[8,64,16]{1,2,0:T(8,128)} %param.26) | copy-start | bytes 98308
  27.6 1.2 copy-start.16
  28.8 0.5 copy-start.17
  30.4 3.8 %copy-start.14 = (f32[8]{0:T(128)}, f32[8]{0:T(128)S(1)}, u32[]{:S(2)}) copy-start(f32[8]{0:T(128)S(1)} %exp.33) | copy-start | bytes 100
  30.4 3.8 %copy-start.15 = (f32[128]{0:T(128)}, f32[128]{0:T(128)S(1)}, u32[]{:S(2)}) copy-start(f32[128]{0:T(128)S(1)} %iota_add_fusion) | copy-start | bytes 1540
  34.2 0.8 copy-start.2
  150.4 2.4 copy-start.4
  159.9 29.0 %copy-start.8 = (f32[8,16,64]{2,1,0:T(8,128)S(1)}, f32[8,16,64]{2,1,0:T(8,128)}, u32[]{:S(2)}) copy-start(f32[8,16,64]{2,1,0:T(8,128)} %param.28) | copy-start | bytes 98308
  159.9 30.8 %copy-start.3 = (f32[8,128,128]{1,2,0:T(8,128)S(1)}, f32[8,128,128]{1,2,0:T(8,128)}, u32[]{:S(2)}) copy-start(f32[8,128,128]{1,2,0:T(8,128)} %copy-done.2) | copy-start | bytes 1572868
  159.9 34.6 %all-to-all-start.2 = ((bf16[16,384,128]{2,1,0:T(8,128)(2,1)}), bf16[16,384,128]{2,1,0:T(8,128)(2,1)S(1)}, u32[]{:S(2)}, u32[]{:S(2)}) async-start(bf16[16,384,128]{2,1,0:T(8,128)(2,1)} %bitcast_bitcast_fusion), calls=%async_computation.2 | async-start | bytes 3145728 | tf_op jit(solution)/shard_map/all_to_all | solution.py:74
  166.8 25.8 %copy-start.9 = (f32[8,16,64]{2,1,0:T(8,128)S(1)}, f32[8,16,64]{2,1,0:T(8,128)}, u32[]{:S(2)}) copy-start(f32[8,16,64]{2,1,0:T(8,128)} %param.27) | copy-start | bytes 98308
  192.6 9.6 %copy-start.18 = (f32[128,2]{0,1:T(2,128)S(1)}, f32[128,2]{0,1:T(2,128)}, u32[]{:S(2)}) copy-start(f32[128,2]{0,1:T(2,128)} %param.36) | copy-start | bytes 3076
  192.7 9.7 %copy-start.13 = (s32[256]{0:T(256)S(1)}, s32[256]{0:T(256)}, u32[]{:S(2)}) copy-start(s32[256]{0:T(256)} %copy-done.12) | copy-start | bytes 3076
  195.4 15.7 %all-to-all-start = ((bf16[16,128,128]{1,2,0:T(8,128)(2,1)}), bf16[16,128,128]{1,2,0:T(8,128)(2,1)S(1)}, u32[]{:S(2)}, u32[]{:S(2)}) async-start(bf16[16,128,128]{1,2,0:T(8,128)(2,1)} %broadcast_in_dim.28), calls=%async_computation | async-start | bytes 1048576 | tf_op jit(solution)/shard_map/all_to_all | solution.py:60
  202.6 28.7 %copy-start.5 = (bf16[2048,128]{1,0:T(8,128)(2,1)S(1)}, bf16[2048,128]{1,0:T(8,128)(2,1)}, u32[]{:S(2)}) copy-start(bf16[2048,128]{1,0:T(8,128)(2,1)} %param.32) | copy-start | bytes 1572868
  211.1 34.6 %all-to-all-start.3 = ((bf16[32,12,128]{2,1,0:T(8,128)(2,1)}), bf16[32,12,128]{2,1,0:T(8,128)(2,1)S(1)}, u32[]{:S(2)}, u32[]{:S(2)}) async-start(bf16[32,12,128]{2,1,0:T(8,128)(2,1)} %reshape.694), calls=%async_computation.3 | async-start | bytes 262144 | tf_op jit(solution)/shard_map/all_to_all | solution.py:242
where the time goes:
time: 249 us; the launch traced here: 247 us
  blocking collectives  99.4 us (40%)
  starting transfers between devices  49.1 us (20%)
  local copies, waits for them, and re-layouts  48.6 us (20%)
  waiting for transfers between devices  21.3 us (9%)
  matrix products  14.1 us (6%)
  other arithmetic  13.8 us (6%)
    all_gather x2, blocking collectives, all_in_one(): both, at, found = (lax.all_gather(jnp.concatenate(lines), axis), 0, {})  99.4 us
    squeeze x50, local copies, waits for them, and re-layouts, entering(): subtotal = combine(subtotal, jax.tree.map(lambda part: part[k], pieces))  31.1 us
    all_to_all x1, starting transfers between devices, local(): lax.all_to_all(final_result, EP, split_axis=0, concat_axis=0, tiled=True)  18.8 us
    all_to_all x1, starting transfers between devices, local(): lax.all_to_all(outgoing, EP, split_axis=0, concat_axis=0, tiled=True)  16.7 us
    all_to_all x1, waiting for transfers between devices, local(): lax.all_to_all(final_result, EP, split_axis=0, concat_axis=0, tiled=True)  13.5 us
    all_to_all x1, waiting for transfers between devices, from_everyone(): return lax.all_to_all(copies, axis, split_axis=0, concat_axis=0, tiled=True)  7.78 us
    all_to_all x1, starting transfers between devices, sent_and_summed(): lax.all_to_all(pieces, axis, split_axis=0, concat_axis=0, tiled=True)  6.89 us
    all_to_all x1, starting transfers between devices, from_everyone(): return lax.all_to_all(copies, axis, split_axis=0, concat_axis=0, tiled=True)  6.65 us
  transfers between devices with their start and end apart: 4, of which 2 were waited for; matrix products, arithmetic and copies ran while one was open for 22% of the time, Pallas kernels for 0%

commit v1 on v0

v1 whole, which is shorter than its diff:
```python
import functools

import jax
import jax.numpy as jnp
from jax import lax
from jax.experimental import pallas as pl
from jax.experimental.pallas import tpu as pltpu
from jax.sharding import Mesh
from jax.sharding import PartitionSpec as P

EP = ("z", "c")
TP = ("y", "x")
MESH = pl.DeviceIdType.MESH
PAD = 16
LANES = 128


EPS = 1e-06
HIGHEST = lax.Precision.HIGHEST


def root_mean_normed(values, gain):
    broadened_rows = values.astype(jnp.float32)
    inverse = lax.rsqrt(jnp.mean(broadened_rows * broadened_rows, axis=-1, keepdims=True) + EPS)
    return (broadened_rows * inverse * gain).astype(jnp.bfloat16)


def discretize(lam_re, lam_im, log_dt, b_re, b_im):
    time_step = jnp.exp(log_dt)[:, None]
    log_mag = lam_re * time_step
    angle = lam_im * time_step
    half_sine = jnp.sin(0.5 * angle)
    minus_re = jnp.expm1(log_mag) * jnp.cos(angle) - 2.0 * half_sine * half_sine
    minus_im = jnp.exp(log_mag) * jnp.sin(angle)
    denom = lam_re * lam_re + lam_im * lam_im
    coef_re = (minus_re * lam_re + minus_im * lam_im) / denom
    coef_im = (minus_im * lam_re - minus_re * lam_im) / denom
    drive_re = coef_re[..., None] * b_re - coef_im[..., None] * b_im
    drive_im = coef_re[..., None] * b_im + coef_im[..., None] * b_re
    return (log_mag, angle, drive_re, drive_im)


def block_scan(inputs, retain, log_mag, angle, drive_re, drive_im):
    length = inputs.shape[0]
    groups, states, channels = drive_re.shape
    broadened_rows = inputs.astype(jnp.float32).reshape(length, groups, channels)
    push_re = jnp.einsum("tgn,gpn->gtp", broadened_rows, drive_re, precision=HIGHEST)
    push_im = jnp.einsum("tgn,gpn->gtp", broadened_rows, drive_im, precision=HIGHEST)
    steps = jnp.arange(length, dtype=jnp.float32)
    causal = steps[:, None] >= steps[None, :]
    summed = jnp.dot(causal.astype(jnp.float32), retain, precision=HIGHEST)
    rows = summed.T
    gaps = jnp.minimum(rows[:, :, None] - rows[:, None, :], 0.0)
    kept = jnp.where(causal[None], jnp.exp(gaps), 0.0)
    centred = (steps - length // 2)[None, :, None]
    growth = log_mag[:, None, :] * centred
    turn = angle[:, None, :] * centred
    cosine = jnp.cos(turn)
    sine = jnp.sin(turn)
    up_re = jnp.exp(growth) * cosine
    up_im = jnp.exp(growth) * sine
    down_re = jnp.exp(-growth) * cosine
    down_im = -jnp.exp(-growth) * sine
    seed_re = push_re * down_re - push_im * down_im
    seed_im = push_re * down_im + push_im * down_re
    seeds = jnp.concatenate([seed_re, seed_im], axis=2)
    held = jnp.einsum("gts,gsp->gtp", kept, seeds, precision=HIGHEST)
    fade = jnp.exp(rows)[:, :, None]
    return (held[..., :states], held[..., states:], up_re, up_im, fade)


def power_of(log_mag, angle, exponent):
    magnitude = jnp.exp(log_mag * exponent)
    return (magnitude * jnp.cos(angle * exponent), magnitude * jnp.sin(angle * exponent))


def cols(index):
    return pl.ds(pl.multiple_of(index * LANES, LANES), LANES)


def exchange_kernel(
    sizes,
    target_ref,
    moe_ref,
    gain_ref,
    blend_ref,
    message_ref,
    turn_ref,
    partial_ref,
    prefix_ref,
    out_re_ref,
    out_im_ref,
    gate_hbm,
    up_hbm,
    down_hbm,
    lin_hbm,
    glu_hbm,
    mix_ref,
    moe_out_ref,
    gate_w,
    up_w,
    down_w,
    mix_w,
    outgoing,
    incoming,
    carries,
    gathered,
    parts,
    first_a,
    first_b,
    sum_a,
    sum_b,
    second_a,
    second_b,
    going_back,
    returned,
    active,
    weight_sem,
    z_sem,
    act_sem,
    ag_recv,
    ag_send,
    rs_sem,
):
    nz, nc, ny, nx, cap = sizes
    experts = nz * nc
    tp = ny * nx
    slots = experts * cap
    half = slots // 2
    mz, mc = lax.axis_index("z"), lax.axis_index("c")
    my, mx = lax.axis_index("y"), lax.axis_index("x")
    me = mz * nc + mc
    mt = my * nx + mx

    def along_z(k):
        peer = lax.rem(me + k, experts)
        return {"z": lax.div(peer, nc), "c": lax.rem(peer, nc)}

    def in_plane(k):
        peer = lax.rem(mt + k, tp)
        return {"y": lax.div(peer, nx), "x": lax.rem(peer, nx)}

    barrier = pltpu.get_barrier_semaphore()

    @pl.loop(1, experts)
    def _(k):
        pl.semaphore_signal(barrier, inc=1, device_id=along_z(k), device_id_type=MESH)

    @pl.loop(1, tp)
    def _(k):
        pl.semaphore_signal(barrier, inc=1, device_id=in_plane(k), device_id_type=MESH)

    loads = [
        pltpu.make_async_copy(gate_hbm, gate_w, weight_sem.at[0]),
        pltpu.make_async_copy(up_hbm, up_w, weight_sem.at[1]),
        pltpu.make_async_copy(down_hbm, down_w, weight_sem.at[2]),
        pltpu.make_async_copy(lin_hbm, mix_w.at[:, pl.ds(0, LANES)], weight_sem.at[3]),
        pltpu.make_async_copy(glu_hbm, mix_w.at[:, pl.ds(LANES, LANES)], weight_sem.at[4]),
    ]
    for load in loads:
        load.start()

    tokens, width = moe_ref.shape
    squares = jnp.zeros((tokens, LANES), jnp.float32)
    for f in range(tp):
        piece = moe_ref[:, f * LANES : (f + 1) * LANES].astype(jnp.float32)
        squares = squares + piece * piece
    mean = jnp.sum(squares, axis=1, keepdims=True) / width
    own = moe_ref[:, cols(mt)].astype(jnp.float32)
    normed = (own * lax.rsqrt(mean + EPS) * gain_ref[:, cols(mt)]).astype(jnp.bfloat16)
    place = lax.broadcasted_iota(jnp.int32, (experts * PAD, tokens), 0)
    picked = (place == target_ref[0:1, :]) | (place == target_ref[1:2, :])
    chosen = jnp.dot(
        picked.astype(jnp.float32).astype(jnp.bfloat16), normed, preferred_element_type=jnp.float32
    )
    outgoing[...] = chosen.astype(jnp.bfloat16).reshape(experts, PAD, LANES)
    incoming[me] = outgoing[me]
    pl.semaphore_wait(barrier, experts + tp - 2)

    def to_expert(k):
        peer = along_z(k)
        return pltpu.make_async_remote_copy(
            src_ref=outgoing.at[peer["z"] * nc + peer["c"]],
            dst_ref=incoming.at[me],
            send_sem=z_sem.at[0],
            recv_sem=z_sem.at[1],
            device_id=peer,
            device_id_type=MESH,
        )

    def to_later(k):
        return pltpu.make_async_remote_copy(
            src_ref=message_ref,
            dst_ref=carries.at[me],
            send_sem=z_sem.at[2],
            recv_sem=z_sem.at[3],
            device_id=along_z(k),
            device_id_type=MESH,
        )

    @pl.loop(1, experts)
    def _(k):
        to_expert(k).start()

    @pl.loop(1, experts)
    def _(k):
        to_later(k).start()

    def settle(ref, sem):
        pltpu.make_async_copy(ref, ref, sem).wait()

    others = pl.ds(0, experts - 1)
    settle(incoming.at[others], z_sem.at[1])

    row = lax.broadcasted_iota(jnp.int32, (slots, experts * PAD), 0)
    column = lax.broadcasted_iota(jnp.int32, (slots, experts * PAD), 1)
    origin = lax.shift_right_logical(row * 5462, 16)
    packing = column == origin * PAD + (row - origin * cap)
    packed = jnp.dot(
        packing.astype(jnp.float32).astype(jnp.bfloat16),
        incoming[...].reshape(experts * PAD, LANES),
        preferred_element_type=jnp.float32,
    ).astype(jnp.bfloat16)
    gathered[:, cols(mt)] = packed

    rows_a, rows_b = pl.ds(0, half), pl.ds(half, half)

    def piece_to(side, source, peer, at):
        rows = rows_a if side == 0 else rows_b
        block = gathered.at[rows, cols(source)]
        return pltpu.make_async_remote_copy(
            src_ref=block,
            dst_ref=block,
            send_sem=ag_send.at[at],
            recv_sem=ag_recv.at[side, source],
            device_id=peer,
            device_id_type=MESH,
        )

    sent = []
    for k in range(1, nx):
        sent.append(piece_to(0, mt, {"x": lax.rem(mx + k, nx)}, len(sent)))
        sent[-1].start()
    for k in range(1, ny):
        sent.append(piece_to(1, mt, {"y": lax.rem(my + k, ny)}, len(sent)))
        sent[-1].start()

    def forward(side, source):
        if side == 0:
            peers = [{"y": lax.rem(my + k, ny)} for k in range(1, ny)]
        else:
            peers = [{"x": lax.rem(mx + k, nx)} for k in range(1, nx)]
        for peer in peers:
            sent.append(piece_to(side, source, peer, len(sent)))
            sent[-1].start()

    forward(0, mt)
    forward(1, mt)
    for k in range(1, max(nx, ny)):
        if k < nx:
            source = my * nx + lax.rem(mx + k, nx)
            piece_to(0, source, {"x": mx}, 0).wait_recv()
            forward(0, source)
        if k < ny:
            source = lax.rem(my + k, ny) * nx + mx
            piece_to(1, source, {"y": my}, 0).wait_recv()
            forward(1, source)

    settle(carries.at[others], z_sem.at[3])
    stay, swap = turn_ref[0], turn_ref[1]

    def absorb(j, state):
        turned = stay * state + swap * pltpu.roll(state, 4, 0)
        return jnp.where(j < me, carries[j, 0:8, :] + carries[j, 8:16, :] * turned, state)

    carries[me] = message_ref[...]
    state = lax.fori_loop(0, experts, absorb, jnp.zeros((8, LANES), jnp.float32))
    carry_re = jnp.concatenate([state[i : i + 1, :] for i in range(4)], axis=1)
    carry_im = jnp.concatenate([state[i : i + 1, :] for i in range(4, 8)], axis=1)
    out_re, out_im = out_re_ref[...], out_im_ref[...]
    reading = jnp.concatenate(
        [out_re * carry_re - out_im * carry_im, -(out_re * carry_im + out_im * carry_re)], axis=1
    )
    total = partial_ref[...] + lax.dot_general(
        prefix_ref[...],
        reading,
        (((1,), (1,)), ((), ())),
        precision=HIGHEST,
        preferred_element_type=jnp.float32,
    )
    active[:, cols(mt)] = jax.nn.gelu(total).astype(jnp.bfloat16)

    for k in range(1, ny):
        for j in range(nx):
            source = lax.rem(my + k, ny) * nx + lax.rem(mx + j, nx)
            piece_to(0, source, {"y": my}, 0).wait_recv()
    for k in range(1, nx):
        for j in range(ny):
            source = lax.rem(my + j, ny) * nx + lax.rem(mx + k, nx)
            piece_to(1, source, {"x": mx}, 0).wait_recv()

    for load in loads:
        load.wait()
    gate = jnp.dot(gathered[...], gate_w[...], preferred_element_type=jnp.float32)
    up = jnp.dot(gathered[...], up_w[...], preferred_element_type=jnp.float32)
    hidden = (gate * jax.nn.sigmoid(gate) * up).astype(jnp.bfloat16)
    for at in range(tp // 2):
        down = jnp.dot(
            hidden,
            down_w[:, at * 2 * LANES : (at + 1) * 2 * LANES],
            preferred_element_type=jnp.float32,
        ).astype(jnp.bfloat16)
        for i in range(2):
            f = at * 2 + i
            parts[f // nx, f % nx] = down[:, i * LANES : (i + 1) * LANES]

    def first_to(side, k):
        if side == 0:
            far = lax.rem(mx + k, nx)
            source, target, peer = parts.at[:, far, rows_a], first_a.at[mx], {"x": far}
        else:
            far = lax.rem(my + k, ny)
            source, target, peer = parts.at[far, :, rows_b], first_b.at[my], {"y": far}
        return pltpu.make_async_remote_copy(
            src_ref=source,
            dst_ref=target,
            send_sem=rs_sem.at[0, side, k],
            recv_sem=rs_sem.at[1, side, k],
            device_id=peer,
            device_id_type=MESH,
        )

    def second_to(side, k):
        if side == 0:
            far = lax.rem(my + k, ny)
            source, target, peer = sum_a.at[far], second_a.at[my], {"y": far}
        else:
            far = lax.rem(mx + k, nx)
            source, target, peer = sum_b.at[far], second_b.at[mx], {"x": far}
        return pltpu.make_async_remote_copy(
            src_ref=source,
            dst_ref=target,
            send_sem=rs_sem.at[2, side, k],
            recv_sem=rs_sem.at[3, side, k],
            device_id=peer,
            device_id_type=MESH,
        )

    for k in range(1, max(nx, ny)):
        if k < nx:
            first_to(0, k).start()
        if k < ny:
            first_to(1, k).start()
    for k in range(1, max(nx, ny)):
        if k < nx:
            first_to(0, k).wait_recv()
        if k < ny:
            first_to(1, k).wait_recv()
    for j in range(ny):
        summed = parts[j, mx, 0:half, :].astype(jnp.float32)
        for k in range(1, nx):
            summed = summed + first_a[lax.rem(mx + k, nx), j].astype(jnp.float32)
        sum_a[j] = summed.astype(jnp.bfloat16)
    for k in range(1, ny):
        second_to(0, k).start()
    for j in range(nx):
        summed = parts[my, j, half:slots, :].astype(jnp.float32)
        for k in range(1, ny):
            summed = summed + first_b[lax.rem(my + k, ny), j].astype(jnp.float32)
        sum_b[j] = summed.astype(jnp.bfloat16)
    for k in range(1, nx):
        second_to(1, k).start()

    def active_to(k):
        block = active.at[:, cols(mt)]
        return pltpu.make_async_remote_copy(
            src_ref=block,
            dst_ref=block,
            send_sem=act_sem.at[0],
            recv_sem=act_sem.at[1],
            device_id=in_plane(k),
            device_id_type=MESH,
        )

    @pl.loop(1, tp)
    def _(k):
        active_to(k).start()

    for k in range(1, ny):
        second_to(0, k).wait_recv()
    for k in range(1, nx):
        second_to(1, k).wait_recv()
    result_a = sum_a[my].astype(jnp.float32)
    for k in range(1, ny):
        result_a = result_a + second_a[lax.rem(my + k, ny)].astype(jnp.float32)
    result_b = sum_b[mx].astype(jnp.float32)
    for k in range(1, nx):
        result_b = result_b + second_b[lax.rem(mx + k, nx)].astype(jnp.float32)
    result = jnp.concatenate([result_a, result_b], axis=0).astype(jnp.bfloat16)

    row = lax.broadcasted_iota(jnp.int32, (experts * PAD, slots), 0)
    column = lax.broadcasted_iota(jnp.int32, (experts * PAD, slots), 1)
    origin = lax.shift_right_logical(row, 4)
    slot = row - origin * PAD
    spreading = (slot < cap) & (column == origin * cap + slot)
    spread = jnp.dot(
        spreading.astype(jnp.float32).astype(jnp.bfloat16),
        result,
        preferred_element_type=jnp.float32,
    )
    going_back[...] = spread.astype(jnp.bfloat16).reshape(experts, PAD, LANES)
    returned[me] = going_back[me]

    def to_owner(k):
        peer = along_z(k)
        return pltpu.make_async_remote_copy(
            src_ref=going_back.at[peer["z"] * nc + peer["c"]],
            dst_ref=returned.at[me],
            send_sem=z_sem.at[4],
            recv_sem=z_sem.at[5],
            device_id=peer,
            device_id_type=MESH,
        )

    @pl.loop(1, experts)
    def _(k):
        to_owner(k).start()

    settle(active.at[:, pl.ds(0, (tp - 1) * LANES)], act_sem.at[1])
    mixed = jnp.dot(active[...], mix_w[...], preferred_element_type=jnp.float32)
    mix_ref[...] = (mixed[:, :LANES] * jax.nn.sigmoid(mixed[:, LANES:])).astype(jnp.bfloat16)

    settle(returned.at[others], z_sem.at[5])
    moe_out_ref[...] = jnp.dot(
        blend_ref[...],
        returned[...].reshape(experts * PAD, LANES).astype(jnp.float32),
        precision=HIGHEST,
        preferred_element_type=jnp.float32,
    ).astype(jnp.bfloat16)

    settle(outgoing.at[others], z_sem.at[0])
    settle(carries.at[others], z_sem.at[2])
    settle(going_back.at[others], z_sem.at[4])
    settle(active.at[:, pl.ds(0, (tp - 1) * LANES)], act_sem.at[0])
    for copy in sent:
        copy.wait_send()
    for k in range(1, nx):
        first_to(0, k).wait_send()
        second_to(1, k).wait_send()
    for k in range(1, ny):
        first_to(1, k).wait_send()
        second_to(0, k).wait_send()


def local(
    sizes,
    mix_in,
    mix_gain,
    lam_re,
    lam_im,
    log_dt,
    b_re,
    b_im,
    c_re,
    c_im,
    d_skip,
    log_retain,
    w_lin,
    w_glu,
    moe_in,
    moe_gain,
    routes,
    route_weight,
    w_gate,
    w_up,
    w_down,
):
    nz, nc, ny, nx, capacity = sizes
    experts, tp = nz * nc, ny * nx
    normed = root_mean_normed(mix_in, mix_gain)
    channels_here = d_skip.shape[0]
    own_inputs = lax.dynamic_slice_in_dim(
        normed, lax.axis_index(TP) * channels_here, channels_here, 1
    )
    log_mag, angle, drive_re, drive_im = discretize(lam_re, lam_im, log_dt, b_re, b_im)
    held_re, held_im, up_re, up_im, fade = block_scan(
        own_inputs, log_retain, log_mag, angle, drive_re, drive_im
    )
    length = own_inputs.shape[0]
    groups, states = log_mag.shape
    local_re = up_re * held_re - up_im * held_im
    local_im = up_re * held_im + up_im * held_re
    states_both = jnp.concatenate([local_re, local_im], axis=2)
    c_both = jnp.concatenate([c_re, -c_im], axis=2)
    read = jnp.einsum("gtp,gnp->tgn", states_both, c_both, precision=HIGHEST)
    partial = read.reshape(length, channels_here) + d_skip * own_inputs.astype(jnp.float32)
    lead_re, lead_im = power_of(log_mag, angle, float(length // 2 + 1))
    pref_re = fade * (up_re * lead_re[:, None] - up_im * lead_im[:, None])
    pref_im = fade * (up_re * lead_im[:, None] + up_im * lead_re[:, None])
    prefix = jnp.concatenate([pref_re, pref_im], axis=0).transpose(1, 0, 2).reshape(length, -1)
    same = jnp.eye(groups, dtype=jnp.float32)[:, None, :, None]
    out_re = (same * c_re[:, :, None, :]).reshape(channels_here, groups * states)
    out_im = (same * c_im[:, :, None, :]).reshape(channels_here, groups * states)
    whole_re, whole_im = power_of(log_mag, angle, float(length))
    lost = jnp.broadcast_to(fade[:, -1], log_mag.shape).reshape(4, LANES)
    message = jnp.concatenate(
        [local_re[:, -1].reshape(4, LANES), local_im[:, -1].reshape(4, LANES), lost, lost], axis=0
    )
    whole_re, whole_im = whole_re.reshape(4, LANES), whole_im.reshape(4, LANES)
    turn = jnp.stack(
        [
            jnp.concatenate([whole_re, whole_re], axis=0),
            jnp.concatenate([-whole_im, whole_im], axis=0),
        ]
    )

    tokens_here, choices_each = routes.shape
    flat_routes = routes.reshape(-1)
    onehot = (flat_routes[:, None] == jnp.arange(experts, dtype=jnp.int32)[None, :]).astype(
        jnp.int32
    )
    earlier_count = jnp.cumsum(onehot, axis=0) - onehot
    slot_index = jnp.sum(earlier_count * onehot, axis=1)
    target = (flat_routes * PAD + slot_index).reshape(tokens_here, choices_each)
    places = jnp.arange(experts * PAD, dtype=jnp.int32)
    blend = jnp.sum(
        jnp.where(target[:, :, None] == places[None, None], route_weight[:, :, None], 0.0), axis=1
    )

    slots, half, width = experts * capacity, experts * capacity // 2, tp * LANES
    hidden_here = w_gate.shape[2]
    bf16 = jnp.bfloat16
    vmem = pl.BlockSpec(memory_space=pltpu.VMEM)
    hbm = pl.BlockSpec(memory_space=pl.ANY)
    return pl.pallas_call(
        functools.partial(exchange_kernel, sizes),
        out_shape=(
            jax.ShapeDtypeStruct((length, LANES), bf16),
            jax.ShapeDtypeStruct((tokens_here, LANES), bf16),
        ),
        in_specs=[vmem] * 10 + [hbm] * 5,
        out_specs=(vmem, vmem),
        scratch_shapes=[
            pltpu.VMEM((width, hidden_here), bf16),
            pltpu.VMEM((width, hidden_here), bf16),
            pltpu.VMEM((hidden_here, width), bf16),
            pltpu.VMEM((width, 2 * LANES), bf16),
            pltpu.VMEM((experts, PAD, LANES), bf16),
            pltpu.VMEM((experts, PAD, LANES), bf16),
            pltpu.VMEM((experts, 16, LANES), jnp.float32),
            pltpu.VMEM((slots, width), bf16),
            pltpu.VMEM((ny, nx, slots, LANES), bf16),
            pltpu.VMEM((nx, ny, half, LANES), bf16),
            pltpu.VMEM((ny, nx, half, LANES), bf16),
            pltpu.VMEM((ny, half, LANES), bf16),
            pltpu.VMEM((nx, half, LANES), bf16),
            pltpu.VMEM((ny, half, LANES), bf16),
            pltpu.VMEM((nx, half, LANES), bf16),
            pltpu.VMEM((experts, PAD, LANES), bf16),
            pltpu.VMEM((experts, PAD, LANES), bf16),
            pltpu.VMEM((length, width), bf16),
            pltpu.SemaphoreType.DMA((5,)),
            pltpu.SemaphoreType.DMA((6,)),
            pltpu.SemaphoreType.DMA((2,)),
            pltpu.SemaphoreType.DMA((2, tp)),
            pltpu.SemaphoreType.DMA((nx - 1 + ny - 1 + nx * (ny - 1) + ny * (nx - 1),)),
            pltpu.SemaphoreType.DMA((4, 2, max(nx, ny))),
        ],
        compiler_params=pltpu.CompilerParams(
            collective_id=0, has_side_effects=True, vmem_limit_bytes=56 * 1024 * 1024
        ),
    )(
        target.T,
        moe_in,
        moe_gain.reshape(1, -1),
        blend,
        message,
        turn,
        partial,
        prefix,
        out_re,
        out_im,
        w_gate[0],
        w_up[0],
        w_down[0],
        w_lin,
        w_glu,
    )


def solution(mesh, sizes=(16, 2, 4, 4, 12)):
    torus = Mesh(mesh.devices.reshape(sizes[:4]), ("z", "c", "y", "x"))
    placed = (
        P(EP, None),
        P(),
        P(TP, None),
        P(TP, None),
        P(TP),
        P(TP, None, None),
        P(TP, None, None),
        P(TP, None, None),
        P(TP, None, None),
        P(TP),
        P(EP, TP),
        P(None, TP),
        P(None, TP),
        P(EP, None),
        P(),
        P(EP, None),
        P(EP, None),
        P(EP, None, TP),
        P(EP, None, TP),
        P(EP, TP, None),
    )
    return jax.shard_map(
        functools.partial(local, sizes),
        mesh=torus,
        in_specs=placed,
        out_specs=(P(EP, TP), P(EP, TP)),
        check_vma=False,
    )
```

time: 249 us -> 97.3 us (0.39)
  blocking collectives: 99.4 us -> 0 us
  Pallas kernels: 0 us -> 74.4 us
  starting transfers between devices: 49.1 us -> 0 us
  local copies, waits for them, and re-layouts: 48.6 us -> 10.5 us
  waiting for transfers between devices: 21.3 us -> 0 us
  matrix products: 14.1 us -> 3.93 us
  other arithmetic: 13.8 us -> 6.67 us
    all_gather x2 -> x0, blocking collectives: 99.4 us -> none  [all_in_one(): both, at, found = (lax.all_gather(jnp.concatenate(lines), axis), 0, {})]
    pallas_call x0 -> x1, Pallas kernels: none -> 74.4 us  [local(): pl.pallas_call(functools.partial(exchange_kernel, sizes), out_shape=(jax....]
    all_to_all x4 -> x0, starting transfers between devices: 49.1 us -> none  [the longest x1 18.8 us: local(): lax.all_to_all(final_result, EP, split_axis=0, concat_axis=0, tiled=True)]
    squeeze x50 -> x0, local copies, waits for them, and re-layouts: 31.1 us -> none  [entering(): subtotal = combine(subtotal, jax.tree.map(lambda part: part[k], pieces))]
    all_to_all x4 -> x0, waiting for transfers between devices: 21.3 us -> none  [the longest x1 13.5 us: local(): lax.all_to_all(final_result, EP, split_axis=0, concat_axis=0, tiled=True)]
    dot_general x6 -> x1, matrix products: 10.9 us -> 0.61 us  [local(): read = jnp.einsum('gtp,gnp->tgn', states_both, c_both, precision=HIGHEST)]
    transpose x1 -> x0, local copies, waits for them, and re-layouts: 2.97 us -> none  [in_blocks(): return jnp.moveaxis(array.reshape(*before, length, -1, *after), dim, 0)]
    reshape x9 -> x4, local copies, waits for them, and re-layouts: 3.98 us -> 1.23 us  [the longest x1 0.99 us: local(): jnp.concatenate([pref_re, pref_im], axis=0).transpose(1, 0, 2)]
  transfers between devices with their start and end apart: 4 -> 0, of which waited for: 2 -> 0; matrix products, arithmetic and copies ran while one was open for 22% -> 0% of each run, Pallas kernels for 0% -> 0%
where the time goes in v1:
time: 97.3 us; the launch traced here: 96.3 us
  Pallas kernels  74.4 us (76%)
  local copies, waits for them, and re-layouts  10.5 us (11%)
  other arithmetic  6.67 us (7%)
  matrix products  3.93 us (4%)
    pallas_call x1, Pallas kernels, local(): pl.pallas_call(functools.partial(exchange_kernel, sizes), out_shape=(jax....  74.4 us
    unnamed x31, local copies, waits for them, and re-layouts  4.97 us

profile of v1, /device:TPU:1, one launch (start us, length us, event | category | flops | bytes accessed | tf_op | source)
XLA Modules:
  0.0 96.3 jit_solution(2094391723842513688)
XLA Ops:
  0.6 0.0 copy-start
  0.7 0.8 dynamic-slice
  1.4 1.2 %convert_element_type.29 = f32[128,2048]{1,0:T(8,128)S(1)} convert(bf16[128,2048]{1,0:T(8,128)(2,1)} %param.20) | non-fusion elementwise | flops 262144 | bytes 1572864 | tf_op jit(solution)/shard_map/convert_element_type | solution.py:23
  2.6 0.0 copy-done.1
  2.6 0.2 multiply_reduce_fusion
  2.8 0.0 copy-start.10
  2.9 0.0 copy-start.5
  2.9 0.1 fusion.43
  3.0 0.0 copy-start.4
  3.0 0.1 copy.41
  3.1 0.0 copy-start.13
  3.1 0.7 copy-done.13
  3.8 0.0 copy-done.9
  3.8 0.0 copy-done.10
  3.8 0.2 cosine_multiply_fusion
  3.9 0.0 copy-done.5
  3.9 0.0 copy-done.4
  3.9 0.4 fusion.51
  4.4 0.0 copy-done
  4.4 0.1 convolution_bitcast_fusion
  4.5 0.1 iota_add_fusion
  4.6 1.4 %fusion.27 = (f32[8,128,64]{1,2,0:T(8,128)S(1)}, f32[8,128,64]{1,2,0:T(8,128)S(1)}, f32[8,128,64]{1,2,0:T(8,128)S(1)}, f32[8,128,64]{1,2,0:T(8,128)S(1)}) fusion(f32[8,64]{1,0:T(8,128)S(1)} %get-tuple-element.13, f32[8,64]{1,0:T(8,128)S(1)} %get-tuple-element.10, f32[8,128]{1,0:T(8,128)S(1)} %get-tuple-element.20, f32[8,64]{1,0:T(8,128)S(1)} %get-tuple-element.16, ...), kind=kOutput, calls=%fused_computation.36 | convolution fusion | flops 14049280 | bytes 1425920 | tf_op jit(solution)/shard_map/tgn,gpn->gtp/dot_general | solution.py:48
  6.1 1.0 %copy.44.prefix_ref = f32[128,1024]{1,0:T(8,128)} copy(f32[128,1024]{0,1:T(8,128)S(1)} %bitcast.46) | data formatting | bytes 1048576 | tf_op jit(solution)/shard_map/reshape | solution.py:500
  7.1 1.3 %fusion = f32[8,128,128]{1,2,0:T(8,128)S(1)} fusion(f32[8,128,64]{1,2,0:T(8,128)S(1)} %get-tuple-element.8, f32[8,128,64]{1,2,0:T(8,128)S(1)} %get-tuple-element.9, f32[8,128]{1,0:T(8,128)S(1)} %convolution_bitcast_fusion, pred[128,128]{1,0:T(8,128)(4,1)S(1)} %iota_compare_fusion.1), kind=kOutput, calls=%fused_computation.2 | convolution fusion | flops 201850880 | bytes 1069056 | tf_op jit(solution)/shard_map/gts,gsp->gtp/dot_general | solution.py:67
  8.5 1.2 %fusion.24 = (f32[8,128,64]{1,2,0:T(8,128)S(1)}, f32[8,128,64]{1,2,0:T(8,128)S(1)}) fusion(f32[8,128,128]{1,2,0:T(8,128)S(1)} %fusion, f32[8,64]{1,0:T(8,128)S(1)} %get-tuple-element.16, f32[128]{0:T(128)S(1)} %iota_add_fusion, f32[8,64]{1,0:T(8,128)S(1)} %get-tuple-element.17), kind=kLoop, calls=%fused_computation.33 | loop fusion | flops 655360 | bytes 1053184 | tf_op jit(solution)/shard_map/sub | solution.py:491
  9.7 0.0 copy-done.2
  9.7 0.0 copy-start.3
  9.7 0.8 copy-done.3
  10.5 0.6 fusion.4
  11.1 0.0 copy-start.12
  11.1 0.1 copy.43
  11.2 0.6 copy-done.12
  11.8 0.7 multiply_add_fusion.partial_ref
  12.5 0.4 slice_reduce_fusion
  12.9 0.1 reshape_squeeze.6
  13.0 0.1 reshape_squeeze.7
  13.0 0.2 slice_reduce_fusion.3
  13.2 0.1 broadcast_in_dim.30
  13.3 0.1 broadcast_in_dim.31
  13.4 0.1 broadcast_in_dim.32
  13.5 0.6 pad_maximum_fusion.1.message_ref
  14.1 0.1 reshape.112
  14.2 0.1 reshape.111
  14.2 0.6 pad_maximum_fusion.2.turn_ref
  14.9 0.1 copy-done.8
  14.9 0.1 copy.37
  15.0 0.1 eq.51
  15.2 0.6 reduce-window.6
  15.8 0.2 slice_reduce_fusion.2
  16.0 0.1 eq.47
  16.2 0.1 fusion.57
  16.3 0.1 reduce_sum.30
  16.4 0.1 copy.40
  16.5 0.7 copy-done.11
  17.2 0.8 select_reduce_fusion.blend_ref
  18.0 0.0 copy-done.7
  18.0 0.2 broadcast_multiply_fusion
  18.2 0.9 mul.361.out_re_ref
  19.1 0.9 mul.364.out_im_ref
  20.0 74.4 %shard_map.203 = (bf16[128,128]{1,0:T(8,128)(2,1)}, bf16[128,128]{1,0:T(8,128)(2,1)}) custom-call(s32[2,128]{1,0:T(2,128)} %bitcast.53, bf16[128,2048]{1,0:T(8,128)(2,1)} %moe_ref.1, f32[1,2048]{1,0:T(1,128)} %bitcast.54, f32[128,512]{1,0:T(8,128)} %select_reduce_fusion.blend_ref, f32[16,128]{1,0:T(8,128)} %pad_maximum_fusion.1.message_ref, ...), custom_call_target="tpu_custom_call" | custom-call | tf_op jit(solution)/shard_map/pallas_call | solution.py:535
  94.3 0.0 copy-start.6
  94.3 1.4 %copy.50 = bf16[128,128]{1,0:T(8,128)(2,1)} copy(bf16[128,128]{1,0:T(8,128)(2,1)} %get-tuple-element.28) | data formatting | bytes 65536
  95.7 0.0 copy-done.6
  95.7 0.6 copy.51
  (19 shorter events, 0.2 us)
Async XLA Ops:
  0.6 3.7 %copy-start = (f32[128,8]{0,1:T(8,128)S(1)}, f32[128,8]{0,1:T(8,128)}, u32[]{:S(2)}) copy-start(f32[128,8]{0,1:T(8,128)} %param.30) | copy-start | bytes 12292
  1.4 1.2 %copy-start.1 = (bf16[128,2048]{1,0:T(8,128)(2,1)S(1)}, bf16[128,2048]{1,0:T(8,128)(2,1)}, u32[]{:S(2)}) copy-start(bf16[128,2048]{1,0:T(8,128)(2,1)} %param.20) | copy-start | bytes 1572868
  2.8 0.9 copy-start.9
  2.8 0.9 copy-start.10
  2.9 1.1 %copy-start.5 = (f32[8,64,16]{1,2,0:T(8,128)S(1)}, f32[8,64,16]{1,2,0:T(8,128)}, u32[]{:S(2)}) copy-start(f32[8,64,16]{1,2,0:T(8,128)} %param.25) | copy-start | bytes 98308
  3.0 1.0 %copy-start.4 = (f32[8,64,16]{1,2,0:T(8,128)S(1)}, f32[8,64,16]{1,2,0:T(8,128)}, u32[]{:S(2)}) copy-start(f32[8,64,16]{1,2,0:T(8,128)} %param.26) | copy-start | bytes 98308
  3.1 0.7 copy-start.13
  8.4 1.2 %copy-start.2 = (f32[8,16,64]{2,1,0:T(8,128)S(1)}, f32[8,16,64]{2,1,0:T(8,128)}, u32[]{:S(2)}) copy-start(f32[8,16,64]{2,1,0:T(8,128)} %param.28) | copy-start | bytes 98308
  9.7 0.8 copy-start.3
  11.1 0.7 copy-start.12
  14.2 0.7 copy-start.8
  16.5 0.7 copy-start.11
  17.2 0.8 copy-start.7
  94.3 1.4 %copy-start.6 = (bf16[128,128]{1,0:T(8,128)(2,1)S(1)}, bf16[128,128]{1,0:T(8,128)(2,1)}, u32[]{:S(2)}) copy-start(bf16[128,128]{1,0:T(8,128)(2,1)} %get-tuple-element.29) | copy-start | bytes 98308

commit v2 on v1

--- a/solution.py
+++ b/solution.py
@@ -19,59 +19,27 @@
 HIGHEST = lax.Precision.HIGHEST
 
 
-def root_mean_normed(values, gain):
-    broadened_rows = values.astype(jnp.float32)
-    inverse = lax.rsqrt(jnp.mean(broadened_rows * broadened_rows, axis=-1, keepdims=True) + EPS)
-    return (broadened_rows * inverse * gain).astype(jnp.bfloat16)
-
-
-def discretize(lam_re, lam_im, log_dt, b_re, b_im):
+def compact_terms(lam_re, lam_im, log_dt, b_re, b_im, c_re, c_im):
     time_step = jnp.exp(log_dt)[:, None]
     log_mag = lam_re * time_step
     angle = lam_im * time_step
     half_sine = jnp.sin(0.5 * angle)
-    minus_re = jnp.expm1(log_mag) * jnp.cos(angle) - 2.0 * half_sine * half_sine
-    minus_im = jnp.exp(log_mag) * jnp.sin(angle)
+    cosine, sine = jnp.cos(angle), jnp.sin(angle)
+    minus_re = jnp.expm1(log_mag) * cosine - 2.0 * half_sine * half_sine
+    minus_im = jnp.exp(log_mag) * sine
     denom = lam_re * lam_re + lam_im * lam_im
     coef_re = (minus_re * lam_re + minus_im * lam_im) / denom
     coef_im = (minus_im * lam_re - minus_re * lam_im) / denom
-    drive_re = coef_re[..., None] * b_re - coef_im[..., None] * b_im
-    drive_im = coef_re[..., None] * b_im + coef_im[..., None] * b_re
-    return (log_mag, angle, drive_re, drive_im)
-
-
-def block_scan(inputs, retain, log_mag, angle, drive_re, drive_im):
-    length = inputs.shape[0]
-    groups, states, channels = drive_re.shape
-    broadened_rows = inputs.astype(jnp.float32).reshape(length, groups, channels)
-    push_re = jnp.einsum("tgn,gpn->gtp", broadened_rows, drive_re, precision=HIGHEST)
-    push_im = jnp.einsum("tgn,gpn->gtp", broadened_rows, drive_im, precision=HIGHEST)
-    steps = jnp.arange(length, dtype=jnp.float32)
-    causal = steps[:, None] >= steps[None, :]
-    summed = jnp.dot(causal.astype(jnp.float32), retain, precision=HIGHEST)
-    rows = summed.T
-    gaps = jnp.minimum(rows[:, :, None] - rows[:, None, :], 0.0)
-    kept = jnp.where(causal[None], jnp.exp(gaps), 0.0)
-    centred = (steps - length // 2)[None, :, None]
-    growth = log_mag[:, None, :] * centred
-    turn = angle[:, None, :] * centred
-    cosine = jnp.cos(turn)
-    sine = jnp.sin(turn)
-    up_re = jnp.exp(growth) * cosine
-    up_im = jnp.exp(growth) * sine
-    down_re = jnp.exp(-growth) * cosine
-    down_im = -jnp.exp(-growth) * sine
-    seed_re = push_re * down_re - push_im * down_im
-    seed_im = push_re * down_im + push_im * down_re
-    seeds = jnp.concatenate([seed_re, seed_im], axis=2)
-    held = jnp.einsum("gts,gsp->gtp", kept, seeds, precision=HIGHEST)
-    fade = jnp.exp(rows)[:, :, None]
-    return (held[..., :states], held[..., states:], up_re, up_im, fade)
-
-
-def power_of(log_mag, angle, exponent):
-    magnitude = jnp.exp(log_mag * exponent)
-    return (magnitude * jnp.cos(angle * exponent), magnitude * jnp.sin(angle * exponent))
+    groups, states, channels = b_re.shape
+    rows = groups * channels
+    flip = (0, 2, 1)
+    drive_re = (coef_re[..., None] * b_re - coef_im[..., None] * b_im).transpose(flip)
+    drive_im = (coef_re[..., None] * b_im + coef_im[..., None] * b_re).transpose(flip)
+    drive = jnp.concatenate([drive_re, drive_im], axis=2).reshape(rows, 2 * states)
+    read = jnp.concatenate([c_re, -c_im], axis=2).reshape(rows, 2 * states)
+    grown, shrunk = jnp.exp(log_mag), jnp.exp(-log_mag)
+    decay = jnp.stack([grown * cosine, grown * sine, shrunk * cosine, -shrunk * sine])
+    return drive, read, jnp.concatenate([decay, decay], axis=2)
 
 
 def cols(index):
@@ -80,16 +48,17 @@
 
 def exchange_kernel(
     sizes,
-    target_ref,
+    routes_ref,
+    weight_ref,
     moe_ref,
-    gain_ref,
-    blend_ref,
-    message_ref,
-    turn_ref,
-    partial_ref,
-    prefix_ref,
-    out_re_ref,
-    out_im_ref,
+    moe_gain_ref,
+    mix_gain_ref,
+    retain_ref,
+    decay_ref,
+    drive_ref,
+    read_ref,
+    skip_ref,
+    mix_hbm,
     gate_hbm,
     up_hbm,
     down_hbm,
@@ -101,6 +70,12 @@
     up_w,
     down_w,
     mix_w,
+    mix_in,
+    blend,
+    powers,
+    partial,
+    fading,
+    message,
     outgoing,
     incoming,
     carries,
@@ -142,14 +117,22 @@
 
     barrier = pltpu.get_barrier_semaphore()
 
-    @pl.loop(1, experts)
+    reach = experts // 2
+
+    @pl.loop(0, reach)
     def _(k):
-        pl.semaphore_signal(barrier, inc=1, device_id=along_z(k), device_id_type=MESH)
+        pl.semaphore_signal(barrier, inc=1, device_id=along_z(reach + k), device_id_type=MESH)
+
+        @pl.when(k > 0)
+        def _():
+            pl.semaphore_signal(barrier, inc=1, device_id=along_z(reach - k), device_id_type=MESH)
 
     @pl.loop(1, tp)
     def _(k):
         pl.semaphore_signal(barrier, inc=1, device_id=in_plane(k), device_id_type=MESH)
 
+    mix_load = pltpu.make_async_copy(mix_hbm, mix_in, weight_sem.at[5])
+    mix_load.start()
     loads = [
         pltpu.make_async_copy(gate_hbm, gate_w, weight_sem.at[0]),
         pltpu.make_async_copy(up_hbm, up_w, weight_sem.at[1]),
@@ -160,21 +143,130 @@
     for load in loads:
         load.start()
 
-    tokens, width = moe_ref.shape
-    squares = jnp.zeros((tokens, LANES), jnp.float32)
-    for f in range(tp):
-        piece = moe_ref[:, f * LANES : (f + 1) * LANES].astype(jnp.float32)
-        squares = squares + piece * piece
-    mean = jnp.sum(squares, axis=1, keepdims=True) / width
-    own = moe_ref[:, cols(mt)].astype(jnp.float32)
-    normed = (own * lax.rsqrt(mean + EPS) * gain_ref[:, cols(mt)]).astype(jnp.bfloat16)
+    tokens = moe_ref.shape[0]
+    lane = lax.broadcasted_iota(jnp.int32, (tokens, LANES), 1)
+    picks = [lane == routes_ref[:, k : k + 1] for k in range(2)]
+    named = jnp.where(picks[0] | picks[1], 1.0, 0.0).astype(jnp.bfloat16)
+    ahead = lax.broadcasted_iota(jnp.int32, (tokens, tokens), 0) > lax.broadcasted_iota(
+        jnp.int32, (tokens, tokens), 1
+    )
+    counted = jnp.dot(
+        jnp.where(ahead, 1.0, 0.0).astype(jnp.bfloat16), named, preferred_element_type=jnp.float32
+    )
+    targets = [
+        routes_ref[:, k : k + 1].astype(jnp.float32) * PAD
+        + jnp.sum(jnp.where(picks[k], counted, 0.0), axis=1, keepdims=True)
+        for k in range(2)
+    ]
+    both = jnp.where(lane == 0, targets[0], targets[1])
+    if tokens < LANES:
+        both = jnp.concatenate([both] * (LANES // tokens), axis=0)
+    across = jnp.transpose(both)[:, :tokens].astype(jnp.int32)
+    wide = lax.broadcasted_iota(jnp.int32, (tokens, experts * PAD), 1)
+    blend[...] = sum(
+        jnp.where(wide == targets[k].astype(jnp.int32), weight_ref[:, k : k + 1], 0.0)
+        for k in range(2)
+    )
+
+    def own_features(source, gain_ref):
+        squares = jnp.zeros((source.shape[0], LANES), jnp.float32)
+        for f in range(tp):
+            piece = source[:, f * LANES : (f + 1) * LANES].astype(jnp.float32)
+            squares = squares + piece * piece
+        mean = jnp.sum(squares, axis=1, keepdims=True) / source.shape[1]
+        own = source[:, cols(mt)].astype(jnp.float32)
+        return (own * lax.rsqrt(mean + EPS) * gain_ref[:, cols(mt)]).astype(jnp.bfloat16)
+
     place = lax.broadcasted_iota(jnp.int32, (experts * PAD, tokens), 0)
-    picked = (place == target_ref[0:1, :]) | (place == target_ref[1:2, :])
+    picked = (place == across[0:1, :]) | (place == across[1:2, :])
     chosen = jnp.dot(
-        picked.astype(jnp.float32).astype(jnp.bfloat16), normed, preferred_element_type=jnp.float32
+        jnp.where(picked, 1.0, 0.0).astype(jnp.bfloat16),
+        own_features(moe_ref, moe_gain_ref),
+        preferred_element_type=jnp.float32,
     )
     outgoing[...] = chosen.astype(jnp.bfloat16).reshape(experts, PAD, LANES)
     incoming[me] = outgoing[me]
+
+    mix_load.wait()
+    inputs = own_features(mix_in, mix_gain_ref).astype(jnp.float32)
+    length, groups = inputs.shape[0], decay_ref.shape[1]
+    turn_lane = lax.broadcasted_iota(jnp.int32, (1, LANES), 1)
+    sign = jnp.where(turn_lane < LANES // 2, -1.0, 1.0)
+
+    def times(a, b):
+        return (a[0] * b[0] - a[1] * b[1], a[0] * b[1] + a[1] * b[0])
+
+    grow = [(decay_ref[0], decay_ref[1])]
+    shrink = [(decay_ref[2], decay_ref[3])]
+    for _ in range(7):
+        grow.append(times(grow[-1], grow[-1]))
+        shrink.append(times(shrink[-1], shrink[-1]))
+    sixteen = lax.broadcasted_iota(jnp.int32, (16, LANES), 0)
+
+    def ladder(bases, start, stride, g):
+        low = (jnp.ones((16, LANES), jnp.float32), jnp.zeros((16, LANES), jnp.float32))
+        for i in range(4):
+            on = (sixteen & (1 << i)) > 0
+            row = [part[g : g + 1, :] for part in bases[i]]
+            low = times(low, (jnp.where(on, row[0], 1.0), jnp.where(on, row[1], 0.0)))
+        high = tuple(part[g : g + 1, :] for part in start)
+        step = tuple(part[g : g + 1, :] for part in stride)
+        blocks = []
+        for _ in range(length // 16):
+            blocks.append(times(low, high))
+            high = times(high, step)
+        return [jnp.concatenate([b[i] for b in blocks], axis=0) for i in range(2)]
+
+    later = lax.broadcasted_iota(jnp.int32, (length, length), 0)
+    sooner = lax.broadcasted_iota(jnp.int32, (length, length), 1)
+    causal = later >= sooner
+    summed = jnp.dot(
+        jnp.where(causal, 1.0, 0.0),
+        retain_ref[...],
+        precision=HIGHEST,
+        preferred_element_type=jnp.float32,
+    )
+    summed_across = jnp.transpose(summed)
+    fading[...] = jnp.exp(summed)
+    group_of = lax.shift_right_logical(lax.broadcasted_iota(jnp.int32, (LANES, LANES), 0), 4)
+
+    def reading(states, g):
+        return lax.dot_general(
+            states,
+            jnp.where(group_of == g, read_ref[...], 0.0),
+            (((1,), (1,)), ((), ())),
+            precision=HIGHEST,
+            preferred_element_type=jnp.float32,
+        )
+
+    total = skip_ref[...] * inputs
+    for g in range(groups):
+        at = g * (LANES // groups)
+        push = jnp.dot(
+            inputs,
+            jnp.where(group_of == g, drive_ref[...], 0.0),
+            precision=HIGHEST,
+            preferred_element_type=jnp.float32,
+        )
+        down_re, down_im = ladder(shrink, grow[6], shrink[4], g)
+        seed = push * down_re + pltpu.roll(push, LANES // 2, 1) * (down_im * sign)
+        gap = jnp.minimum(summed[:, at : at + 1] - summed_across[at : at + 1, :], 0.0)
+        kept = jnp.where(causal, jnp.exp(gap), 0.0)
+        held = jnp.dot(kept, seed, precision=HIGHEST, preferred_element_type=jnp.float32)
+        up_re, up_im = ladder(grow, shrink[6], grow[4], g)
+        up_im = up_im * sign
+        powers[0, g] = up_re
+        powers[1, g] = up_im
+        states = held * up_re + pltpu.roll(held, LANES // 2, 1) * up_im
+        total = total + reading(states, g)
+        message[g : g + 1, :] = states[length - 1 : length, :]
+        message[groups + g : groups + g + 1, :] = jnp.broadcast_to(
+            fading[length - 1 : length, at : at + 1], (1, LANES)
+        )
+    partial[...] = total
+    lead = times(grow[6], grow[0])
+    lead = (lead[0], lead[1] * sign)
+    turn = (grow[7][0], grow[7][1] * sign)
     pl.semaphore_wait(barrier, experts + tp - 2)
 
     def to_expert(k):
@@ -190,7 +282,7 @@
 
     def to_later(k):
         return pltpu.make_async_remote_copy(
-            src_ref=message_ref,
+            src_ref=message,
             dst_ref=carries.at[me],
             send_sem=z_sem.at[2],
             recv_sem=z_sem.at[3],
@@ -267,27 +359,23 @@
             forward(1, source)
 
     settle(carries.at[others], z_sem.at[3])
-    stay, swap = turn_ref[0], turn_ref[1]
-
-    def absorb(j, state):
-        turned = stay * state + swap * pltpu.roll(state, 4, 0)
-        return jnp.where(j < me, carries[j, 0:8, :] + carries[j, 8:16, :] * turned, state)
-
-    carries[me] = message_ref[...]
-    state = lax.fori_loop(0, experts, absorb, jnp.zeros((8, LANES), jnp.float32))
-    carry_re = jnp.concatenate([state[i : i + 1, :] for i in range(4)], axis=1)
-    carry_im = jnp.concatenate([state[i : i + 1, :] for i in range(4, 8)], axis=1)
-    out_re, out_im = out_re_ref[...], out_im_ref[...]
-    reading = jnp.concatenate(
-        [out_re * carry_re - out_im * carry_im, -(out_re * carry_im + out_im * carry_re)], axis=1
-    )
-    total = partial_ref[...] + lax.dot_general(
-        prefix_ref[...],
-        reading,
-        (((1,), (1,)), ((), ())),
-        precision=HIGHEST,
-        preferred_element_type=jnp.float32,
-    )
+    carries[me] = message[...]
+    state = crossed = jnp.zeros((groups, LANES), jnp.float32)
+    for j in range(experts):
+        own, left = carries[j, 0:groups, :], carries[j, groups : 2 * groups, :]
+        turned = own + left * (turn[0] * state + turn[1] * crossed)
+        turned_crossed = pltpu.roll(own, LANES // 2, 1) + left * (
+            turn[0] * crossed - turn[1] * state
+        )
+        state = jnp.where(j < me, turned, state)
+        crossed = jnp.where(j < me, turned_crossed, crossed)
+    first = lead[0] * state + lead[1] * crossed
+    first_crossed = lead[0] * crossed - lead[1] * state
+    carried = jnp.zeros((length, LANES), jnp.float32)
+    for g in range(groups):
+        row, row_crossed = first[g : g + 1, :], first_crossed[g : g + 1, :]
+        carried = carried + reading(powers[0, g] * row + powers[1, g] * row_crossed, g)
+    total = partial[...] + fading[...] * carried
     active[:, cols(mt)] = jax.nn.gelu(total).astype(jnp.bfloat16)
 
     for k in range(1, ny):
@@ -432,7 +520,7 @@
 
     settle(returned.at[others], z_sem.at[5])
     moe_out_ref[...] = jnp.dot(
-        blend_ref[...],
+        blend[...],
         returned[...].reshape(experts * PAD, LANES).astype(jnp.float32),
         precision=HIGHEST,
         preferred_element_type=jnp.float32,
@@ -477,56 +565,10 @@
 ):
     nz, nc, ny, nx, capacity = sizes
     experts, tp = nz * nc, ny * nx
-    normed = root_mean_normed(mix_in, mix_gain)
-    channels_here = d_skip.shape[0]
-    own_inputs = lax.dynamic_slice_in_dim(
-        normed, lax.axis_index(TP) * channels_here, channels_here, 1
-    )
-    log_mag, angle, drive_re, drive_im = discretize(lam_re, lam_im, log_dt, b_re, b_im)
-    held_re, held_im, up_re, up_im, fade = block_scan(
-        own_inputs, log_retain, log_mag, angle, drive_re, drive_im
-    )
-    length = own_inputs.shape[0]
-    groups, states = log_mag.shape
-    local_re = up_re * held_re - up_im * held_im
-    local_im = up_re * held_im + up_im * held_re
-    states_both = jnp.concatenate([local_re, local_im], axis=2)
-    c_both = jnp.concatenate([c_re, -c_im], axis=2)
-    read = jnp.einsum("gtp,gnp->tgn", states_both, c_both, precision=HIGHEST)
-    partial = read.reshape(length, channels_here) + d_skip * own_inputs.astype(jnp.float32)
-    lead_re, lead_im = power_of(log_mag, angle, float(length // 2 + 1))
-    pref_re = fade * (up_re * lead_re[:, None] - up_im * lead_im[:, None])
-    pref_im = fade * (up_re * lead_im[:, None] + up_im * lead_re[:, None])
-    prefix = jnp.concatenate([pref_re, pref_im], axis=0).transpose(1, 0, 2).reshape(length, -1)
-    same = jnp.eye(groups, dtype=jnp.float32)[:, None, :, None]
-    out_re = (same * c_re[:, :, None, :]).reshape(channels_here, groups * states)
-    out_im = (same * c_im[:, :, None, :]).reshape(channels_here, groups * states)
-    whole_re, whole_im = power_of(log_mag, angle, float(length))
-    lost = jnp.broadcast_to(fade[:, -1], log_mag.shape).reshape(4, LANES)
-    message = jnp.concatenate(
-        [local_re[:, -1].reshape(4, LANES), local_im[:, -1].reshape(4, LANES), lost, lost], axis=0
-    )
-    whole_re, whole_im = whole_re.reshape(4, LANES), whole_im.reshape(4, LANES)
-    turn = jnp.stack(
-        [
-            jnp.concatenate([whole_re, whole_re], axis=0),
-            jnp.concatenate([-whole_im, whole_im], axis=0),
-        ]
-    )
-
-    tokens_here, choices_each = routes.shape
-    flat_routes = routes.reshape(-1)
-    onehot = (flat_routes[:, None] == jnp.arange(experts, dtype=jnp.int32)[None, :]).astype(
-        jnp.int32
-    )
-    earlier_count = jnp.cumsum(onehot, axis=0) - onehot
-    slot_index = jnp.sum(earlier_count * onehot, axis=1)
-    target = (flat_routes * PAD + slot_index).reshape(tokens_here, choices_each)
-    places = jnp.arange(experts * PAD, dtype=jnp.int32)
-    blend = jnp.sum(
-        jnp.where(target[:, :, None] == places[None, None], route_weight[:, :, None], 0.0), axis=1
-    )
-
+    drive, read, decay = compact_terms(lam_re, lam_im, log_dt, b_re, b_im, c_re, c_im)
+    groups = decay.shape[1]
+    retain = jnp.repeat(log_retain, LANES // groups, axis=1)
+    length, tokens_here = mix_in.shape[0], routes.shape[0]
     slots, half, width = experts * capacity, experts * capacity // 2, tp * LANES
     hidden_here = w_gate.shape[2]
     bf16 = jnp.bfloat16
@@ -538,13 +580,19 @@
             jax.ShapeDtypeStruct((length, LANES), bf16),
             jax.ShapeDtypeStruct((tokens_here, LANES), bf16),
         ),
-        in_specs=[vmem] * 10 + [hbm] * 5,
+        in_specs=[vmem] * 10 + [hbm] * 6,
         out_specs=(vmem, vmem),
         scratch_shapes=[
             pltpu.VMEM((width, hidden_here), bf16),
             pltpu.VMEM((width, hidden_here), bf16),
             pltpu.VMEM((hidden_here, width), bf16),
             pltpu.VMEM((width, 2 * LANES), bf16),
+            pltpu.VMEM((length, width), bf16),
+            pltpu.VMEM((tokens_here, experts * PAD), jnp.float32),
+            pltpu.VMEM((2, groups, length, LANES), jnp.float32),
+            pltpu.VMEM((length, LANES), jnp.float32),
+            pltpu.VMEM((length, LANES), jnp.float32),
+            pltpu.VMEM((2 * groups, LANES), jnp.float32),
             pltpu.VMEM((experts, PAD, LANES), bf16),
             pltpu.VMEM((experts, PAD, LANES), bf16),
             pltpu.VMEM((experts, 16, LANES), jnp.float32),
@@ -559,7 +607,7 @@
             pltpu.VMEM((experts, PAD, LANES), bf16),
             pltpu.VMEM((experts, PAD, LANES), bf16),
             pltpu.VMEM((length, width), bf16),
-            pltpu.SemaphoreType.DMA((5,)),
+            pltpu.SemaphoreType.DMA((6,)),
             pltpu.SemaphoreType.DMA((6,)),
             pltpu.SemaphoreType.DMA((2,)),
             pltpu.SemaphoreType.DMA((2, tp)),
@@ -570,16 +618,17 @@
             collective_id=0, has_side_effects=True, vmem_limit_bytes=56 * 1024 * 1024
         ),
     )(
-        target.T,
+        routes,
+        route_weight,
         moe_in,
         moe_gain.reshape(1, -1),
-        blend,
-        message,
-        turn,
-        partial,
-        prefix,
-        out_re,
-        out_im,
+        mix_gain.reshape(1, -1),
+        retain,
+        decay,
+        drive,
+        read,
+        d_skip.reshape(1, -1),
+        mix_in,
         w_gate[0],
         w_up[0],
         w_down[0],

time: 97.3 us -> 86.6 us (0.89)
  local copies, waits for them, and re-layouts: 10.5 us -> 5.72 us
  matrix products: 3.93 us -> 0 us
  other arithmetic: 6.67 us -> 3.82 us
  Pallas kernels: 74.4 us -> 76 us
    dot_general x5 -> x0, matrix products: 3.93 us -> none  [the longest x1 1.44 us: block_scan(): jnp.einsum('tgn,gpn->gtp', broadened_rows, drive_im, precision=HIGHEST)]
    mul x2 -> x0, local copies, waits for them, and re-layouts: 1.76 us -> none  [the longest x1 0.88 us: local(): same * c_im[:, :, None, :]]
    pallas_call x1, Pallas kernels: 74.4 us -> 76 us  [local(): pl.pallas_call(functools.partial(exchange_kernel, sizes), out_shape=(jax....]
    concatenate x2 -> x3, other arithmetic: 0.66 us -> 2.09 us  [the longest x1 0.71 us: compact_terms(): read = jnp.concatenate([c_re, -c_im], axis=2).reshape(rows, 2 * states)]
    convert_element_type x4 -> x0, other arithmetic: 1.31 us -> none  [the longest x1 1.21 us: root_mean_normed(): broadened_rows = values.astype(jnp.float32)]
    sub x2 -> x0, other arithmetic: 1.27 us -> none  [the longest x1 1.2 us: local(): local_re = up_re * held_re - up_im * held_im]
    another operation x4 -> x0, other arithmetic: 1.24 us -> none
    reduce_sum x3 -> x0, other arithmetic: 1.12 us -> none  [the longest x1 0.84 us: local(): jnp.sum(jnp.where(target[:, :, None] == places[None, None], route_weight[...]
where the time goes in v2:
time: 86.6 us; the launch traced here: 86.2 us
  Pallas kernels  76 us (88%)
  local copies, waits for them, and re-layouts  5.72 us (7%)
  other arithmetic  3.82 us (4%)
    pallas_call x1, Pallas kernels, local(): pl.pallas_call(functools.partial(exchange_kernel, sizes), out_shape=(jax....  76 us
    unnamed x16, local copies, waits for them, and re-layouts  4.33 us

profile of v2, /device:TPU:1, one launch (start us, length us, event | category | flops | bytes accessed | tf_op | source)
XLA Modules:
  0.0 86.2 jit_solution(8465804761285830498)
XLA Ops:
  0.6 0.7 exp.10
  1.3 0.8 fusion.1
  2.1 0.9 %subtract_bitcast_fusion = (f32[8,16,64]{2,1,0:T(8,128)S(1)}, f32[8,16,64]{2,1,0:T(8,128)S(1)}) fusion(f32[8,64,16]{1,2,0:T(8,128)} %param.26, f32[8,64,16]{1,2,0:T(8,128)} %param.25, f32[8,64]{1,0:T(8,128)S(1)} %get-tuple-element.9, f32[8,64]{1,0:T(8,128)S(1)} %get-tuple-element.4), kind=kLoop, calls=%fused_computation.3 | loop fusion | flops 49152 | bytes 135168 | tf_op jit(solution)/shard_map/transpose | solution.py:36
  3.0 0.0 copy-start.1
  3.0 0.7 pad_maximum_fusion
  3.7 0.7 maximum_maximum_fusion.decay_ref
  4.4 0.0 copy-done.1
  4.4 0.0 copy-start
  4.4 0.8 copy-done
  5.3 0.0 copy-start.3
  5.3 0.7 pad_maximum_fusion.1
  6.0 0.0 copy-done.3
  6.0 0.0 copy-start.4
  6.0 0.7 copy.27.retain_ref
  6.7 0.0 copy-done.4
  6.7 0.0 copy-start.5
  6.7 0.7 copy.25.routes_ref
  7.5 0.0 copy-done.5
  7.5 0.7 copy.26.weight_ref
  8.2 76.0 %shard_map.203 = (bf16[128,128]{1,0:T(8,128)(2,1)}, bf16[128,128]{1,0:T(8,128)(2,1)}) custom-call(s32[128,2]{1,0:T(8,128)} %copy.25.routes_ref, f32[128,2]{1,0:T(8,128)} %copy.26.weight_ref, bf16[128,2048]{1,0:T(8,128)(2,1)} %moe_ref.1, f32[1,2048]{1,0:T(1,128)} %bitcast.27, f32[1,2048]{1,0:T(1,128)} %bitcast.28, f32[128,128]{1,0:T(8,128)} %copy.27.retain_ref, ...), custom_call_target="tpu_custom_call" | custom-call | tf_op jit(solution)/shard_map/pallas_call | solution.py:577
  84.2 0.0 copy-start.2
  84.2 1.4 %copy.30 = bf16[128,128]{1,0:T(8,128)(2,1)} copy(bf16[128,128]{1,0:T(8,128)(2,1)} %get-tuple-element.12) | data formatting | bytes 65536
  85.6 0.0 copy-done.2
  85.6 0.6 copy.31
  (2 shorter events, 0.0 us)
Async XLA Ops:
  3.0 1.4 %copy-start.1 = (f32[8,16,64]{2,1,0:T(8,128)S(1)}, f32[8,16,64]{2,1,0:T(8,128)}, u32[]{:S(2)}) copy-start(f32[8,16,64]{2,1,0:T(8,128)} %param.28) | copy-start | bytes 98308
  4.4 0.8 copy-start
  5.3 0.7 copy-start.3
  6.0 0.7 copy-start.4
  6.7 0.7 copy-start.5
  84.2 1.4 %copy-start.2 = (bf16[128,128]{1,0:T(8,128)(2,1)S(1)}, bf16[128,128]{1,0:T(8,128)(2,1)}, u32[]{:S(2)}) copy-start(bf16[128,128]{1,0:T(8,128)(2,1)} %get-tuple-element.13) | copy-start | bytes 98308
